TPU v7x, 32 devices: a whole 2x2x4 slice. The times are simulated.
32 devices in a mesh: sp: 8 (over z, y), dp: 4 (over x, core).
Axes of the slice: x: 2, y: 2, z: 4, core: 2. Of those that a mesh axis runs over, the one named last changes fastest.
Arguments:
- tokens: bfloat16 [8, 512, 2048], P('dp', 'sp'), may hold values from -6 to 6
- norm_gain: float32 [2048], replicated, may hold values from 0.1 to 1.9
- w_query: bfloat16 [2048, 4096], P(None, 'dp'), may hold values from -1 to 1
- w_key: bfloat16 [2048, 1024], P(None, 'dp'), may hold values from -1 to 1
- w_value: bfloat16 [2048, 1024], P(None, 'dp'), may hold values from -0.125 to 0.125
- break_bias: float32 [32], P('dp'), may hold values from -12 to -3
- w_out: bfloat16 [4096, 2048], P('dp'), may hold values from -0.09375 to 0.09375
Outputs:
- mixed: bfloat16 [8, 512, 2048], P('dp', 'sp')
All inputs are finite; a program needn't handle non-finite values.
Results may differ from a plain program's by a relative error of at most 0.015.
Values may be sent and summed in bfloat16 or wider, within the bound.
A program may use at most 64 MiB of HBM per device.

v0:
```python
import math

import jax
import jax.numpy as jnp
from jax import lax
from jax.sharding import PartitionSpec as P

HEAD_DIM = 128


EPS = 1e-06


def normalize(tokens):
    widened = tokens.astype(jnp.float32)
    return widened * lax.rsqrt(jnp.mean(widened * widened, axis=-1, keepdims=True) + EPS)


def head_major(normed, weight, copies):
    model_width = weight.shape[0]
    head_count = weight.shape[1] // HEAD_DIM
    result = jnp.einsum(
        "ntd,dhc->nhtc",
        normed,
        weight.reshape(model_width, head_count, HEAD_DIM),
        preferred_element_type=jnp.float32,
    ).astype(jnp.bfloat16)
    return jnp.repeat(result, copies, axis=1)


def stick_item(operands):
    query_data, key_data, value_data, bias_term = operands
    seq_length = query_data.shape[0]
    block_size = math.gcd(seq_length, 512)
    head_scale = HEAD_DIM ** (-0.5)
    offsets = jnp.arange(block_size, dtype=jnp.int32)

    def query_block(block_index):
        query_rows = lax.dynamic_slice_in_dim(query_data, block_index * block_size, block_size, 0)
        query_pos = block_index * block_size + offsets

        def key_block(step_count, carry):
            carried, accumulated = carry
            key_index = block_index - step_count
            key_rows = lax.dynamic_slice_in_dim(key_data, key_index * block_size, block_size, 0)
            value_rows = lax.dynamic_slice_in_dim(value_data, key_index * block_size, block_size, 0)
            key_pos = key_index * block_size + offsets
            scores = (
                jnp.einsum("qc,kc->qk", query_rows, key_rows, preferred_element_type=jnp.float32)
                * head_scale
                + bias_term
            )
            causal = key_pos[None, :] < query_pos[:, None]
            log_keep = jnp.where(causal, jax.nn.log_sigmoid(-scores), 0.0)
            after_sum = lax.cumsum(log_keep, axis=1, reverse=True) - log_keep + carried[:, None]
            weights = jnp.where(
                causal, jnp.exp(jax.nn.log_sigmoid(scores) + after_sum), 0.0
            ).astype(jnp.bfloat16)
            accumulated = accumulated + jnp.dot(
                weights, value_rows, preferred_element_type=jnp.float32
            )
            return (carried + jnp.sum(log_keep, axis=1), accumulated)

        initial = (
            jnp.zeros((block_size,), jnp.float32),
            jnp.zeros((block_size, HEAD_DIM), jnp.float32),
        )
        carried, accumulated = lax.fori_loop(0, block_index + 1, key_block, initial)
        return accumulated.astype(jnp.bfloat16)

    blocks = lax.map(query_block, jnp.arange(seq_length // block_size, dtype=jnp.int32))
    return blocks.reshape(seq_length, HEAD_DIM)


def local(tokens, norm_gain, w_query, w_key, w_value, break_bias, w_out):
    own_seqs = tokens.shape[0]
    seq_count = lax.axis_size("dp") * own_seqs
    seq_parts = lax.axis_size("sp")
    local_heads = w_query.shape[1] // HEAD_DIM
    copies = local_heads // (w_key.shape[1] // HEAD_DIM)
    tok_rows = tokens.shape[1]
    model_width = tokens.shape[2]
    item_count = seq_count * local_heads
    normed = (normalize(lax.all_gather(tokens, "dp", axis=0, tiled=True)) * norm_gain).astype(
        jnp.bfloat16
    )
    combined = jnp.concatenate(
        (
            head_major(normed, w_query, 1),
            head_major(normed, w_key, copies),
            head_major(normed, w_value, copies),
        ),
        axis=3,
    )
    arrived = lax.all_to_all(
        combined.reshape(item_count, tok_rows, 3 * HEAD_DIM),
        "sp",
        split_axis=0,
        concat_axis=1,
        tiled=True,
    )
    query_data = arrived[:, :, :HEAD_DIM]
    key_data = arrived[:, :, HEAD_DIM : 2 * HEAD_DIM]
    value_data = arrived[:, :, 2 * HEAD_DIM :]
    per_device = item_count // seq_parts
    item_ids = lax.axis_index("sp") * per_device + jnp.arange(per_device, dtype=jnp.int32)
    local_ids = item_ids % local_heads
    bias_items = jnp.sum(
        jnp.where(
            local_ids[:, None] == jnp.arange(local_heads, dtype=jnp.int32)[None, :],
            break_bias[None, :],
            0.0,
        ),
        axis=1,
    )
    attended = lax.map(stick_item, (query_data, key_data, value_data, bias_items))
    returned = lax.all_to_all(attended, "sp", split_axis=1, concat_axis=0, tiled=True)
    grouped = returned.reshape(seq_count, local_heads, tok_rows, HEAD_DIM)
    out_weight = w_out.reshape(local_heads, HEAD_DIM, model_width)
    term_rows = jnp.einsum(
        "nhtc,hcd->ntd", grouped, out_weight, preferred_element_type=jnp.float32
    ).astype(jnp.bfloat16)
    term_rows = lax.optimization_barrier(term_rows)
    summed = lax.psum_scatter(
        term_rows.astype(jnp.float32).astype(jnp.bfloat16), "dp", scatter_dimension=0, tiled=True
    ).astype(jnp.float32)
    return normalize(summed).astype(jnp.bfloat16)


def solution(mesh):
    return jax.shard_map(
        local,
        mesh=mesh,
        in_specs=(
            P("dp", "sp", None),
            P(),
            P(None, "dp"),
            P(None, "dp"),
            P(None, "dp"),
            P("dp"),
            P("dp", None),
        ),
        out_specs=P("dp", "sp", None),
        check_vma=False,
    )
```

profile of v0, /device:TPU:0, one launch (start us, length us, event | category | flops | bytes accessed | tf_op | source)
XLA Modules:
  0.0 289.7 jit_solution(7165742282092451112)
XLA Ops:
  7.3 26.9 %all-gather.2.cloned.1.call-done = bf16[8,64,2048]{2,1,0:T(8,128)(2,1)} async-done(((bf16[2,64,2048]{2,1,0:T(8,128)(2,1)}), bf16[8,64,2048]{2,1,0:T(8,128)(2,1)}) %all-gather.2.cloned.1.call-update) | async-done | bytes 2097168 | tf_op jit(solution)/shard_map/all_gather | solution.py:84
  34.2 2.2 fusion.20
  36.4 2.4 fusion.27
  39.6 1.4 copy-done.4
  41.0 2.4 fusion.26
  43.9 2.2 pad_maximum_fusion
  46.1 5.6 %all-to-all-start = ((bf16[64,64,384]{2,1,0:T(8,128)(2,1)}), bf16[64,64,384]{2,1,0:T(8,128)(2,1)}, u32[]{:S(2)}, u32[]{:S(2)}) async-start(bf16[64,64,384]{2,1,0:T(8,128)(2,1)} %pad_maximum_fusion), calls=%async_computation | async-start | bytes 6291456 | tf_op jit(solution)/shard_map/all_to_all | solution.py:95
  52.2 70.8 %all-to-all-done = bf16[64,64,384]{2,1,0:T(8,128)(2,1)} async-done(((bf16[64,64,384]{2,1,0:T(8,128)(2,1)}), bf16[64,64,384]{2,1,0:T(8,128)(2,1)}, u32[]{:S(2)}, u32[]{:S(2)}) %all-to-all-start) | async-done | bytes 3145760 | tf_op jit(solution)/shard_map/all_to_all | solution.py:95
  122.9 2.3 copy.34
  125.3 2.2 fusion.37
  127.5 87.6 %while.42 = (s32[]{:T(128)}, bf16[8,512,128]{2,1,0:T(8,128)(2,1)}, bf16[8,512,128]{2,1,0:T(8,128)(2,1)}, bf16[8,512,128]{2,1,0:T(8,128)(2,1)}, bf16[8,512,128]{2...) while((s32[]{:T(128)}, bf16[8,512,128]{2,1,0:T(8,128)(2,1)}, bf16[8,512,128]{2,1,0:T(8,128)(2,1)}, ...), condition=%wide.region_8.9_spmd, body=%wide.region_2.8_spmd.sunk | while | flops 176233984 | bytes 20542108 | solution.py:116
  128.2 2.1 fusion.54
  130.3 4.8 %fusion.55 = f32[512,4,128]{0,1,2:T(4,128)S(1)} fusion(f32[512,4,128]{0,2,1:T(8,128)S(1)} %bitcast.121), kind=kOutput, calls=%fused_computation.15.clone.1 | output fusion | flops 33292288 | bytes 2097152 | tf_op jit(solution)/shard_map/reduce-window.6 | solution.py:68
  135.6 0.9 fusion.56
  136.5 1.9 fusion.57
  139.1 2.1 fusion.54
  141.2 4.8 %fusion.55 = f32[512,4,128]{0,1,2:T(4,128)S(1)} fusion(f32[512,4,128]{0,2,1:T(8,128)S(1)} %bitcast.121), kind=kOutput, calls=%fused_computation.15.clone.1 | output fusion | flops 33292288 | bytes 2097152 | tf_op jit(solution)/shard_map/reduce-window.6 | solution.py:68
  146.6 0.9 fusion.56
  147.5 1.9 fusion.57
  150.1 2.1 fusion.54
  152.2 4.8 %fusion.55 = f32[512,4,128]{0,1,2:T(4,128)S(1)} fusion(f32[512,4,128]{0,2,1:T(8,128)S(1)} %bitcast.121), kind=kOutput, calls=%fused_computation.15.clone.1 | output fusion | flops 33292288 | bytes 2097152 | tf_op jit(solution)/shard_map/reduce-window.6 | solution.py:68
  157.5 0.9 fusion.56
  158.4 1.9 fusion.57
  161.0 2.1 fusion.54
  163.1 4.8 %fusion.55 = f32[512,4,128]{0,1,2:T(4,128)S(1)} fusion(f32[512,4,128]{0,2,1:T(8,128)S(1)} %bitcast.121), kind=kOutput, calls=%fused_computation.15.clone.1 | output fusion | flops 33292288 | bytes 2097152 | tf_op jit(solution)/shard_map/reduce-window.6 | solution.py:68
  168.5 0.9 fusion.56
  169.4 1.9 fusion.57
  172.0 2.1 fusion.54
  174.1 4.8 %fusion.55 = f32[512,4,128]{0,1,2:T(4,128)S(1)} fusion(f32[512,4,128]{0,2,1:T(8,128)S(1)} %bitcast.121), kind=kOutput, calls=%fused_computation.15.clone.1 | output fusion | flops 33292288 | bytes 2097152 | tf_op jit(solution)/shard_map/reduce-window.6 | solution.py:68
  179.4 0.9 fusion.56
  180.3 1.9 fusion.57
  182.9 2.1 fusion.54
  185.0 4.8 %fusion.55 = f32[512,4,128]{0,1,2:T(4,128)S(1)} fusion(f32[512,4,128]{0,2,1:T(8,128)S(1)} %bitcast.121), kind=kOutput, calls=%fused_computation.15.clone.1 | output fusion | flops 33292288 | bytes 2097152 | tf_op jit(solution)/shard_map/reduce-window.6 | solution.py:68
  190.4 0.9 fusion.56
  191.3 1.9 fusion.57
  193.8 2.1 fusion.54
  196.0 4.8 %fusion.55 = f32[512,4,128]{0,1,2:T(4,128)S(1)} fusion(f32[512,4,128]{0,2,1:T(8,128)S(1)} %bitcast.121), kind=kOutput, calls=%fused_computation.15.clone.1 | output fusion | flops 33292288 | bytes 2097152 | tf_op jit(solution)/shard_map/reduce-window.6 | solution.py:68
  201.3 0.9 fusion.56
  202.2 1.9 fusion.57
  204.8 2.1 fusion.54
  206.9 4.8 %fusion.55 = f32[512,4,128]{0,1,2:T(4,128)S(1)} fusion(f32[512,4,128]{0,2,1:T(8,128)S(1)} %bitcast.121), kind=kOutput, calls=%fused_computation.15.clone.1 | output fusion | flops 33292288 | bytes 2097152 | tf_op jit(solution)/shard_map/reduce-window.6 | solution.py:68
  213.1 1.9 fusion.57
  215.1 2.1 copy.35
  217.1 29.3 %all_to_all.33 = bf16[8,512,128]{2,0,1:T(8,128)(2,1)S(1)} all-to-all(bf16[8,512,128]{2,0,1:T(8,128)(2,1)S(1)} %copy.35), channel_id=1, replica_groups=mesh['sp'=8,'dp'=4] {'sp'}, dimensions={1} | all-to-all | bytes 2097152 | tf_op jit(solution)/shard_map/all_to_all | solution.py:117
  246.6 3.6 %bitcast_convert_fusion = bf16[8,64,2048]{2,1,0:T(8,128)(2,1)} fusion(bf16[8,8,64,128]{3,2,0,1:T(8,128)(2,1)S(1)} %bitcast.126, bf16[8,128,2048,1]{2,1,3,0:T(8,128)(2,1)S(1)} %bitcast.128), kind=kOutput, calls=%fused_computation.36 | convolution fusion | flops 2148532224 | bytes 7340032 | tf_op jit(solution)/shard_map/nhtc,hcd->ntd/dot_general | solution.py:120
  250.2 29.4 %reduce-scatter.2.cloned.1.call-done = bf16[2,64,2048]{2,1,0:T(8,128)(2,1)} async-done(((bf16[8,64,2048]{2,1,0:T(8,128)(2,1)}), bf16[2,64,2048]{2,1,0:T(8,128)(2,1)}) %reduce-scatter.2.cloned.1.call-update) | async-done | bytes 524304 | tf_op jit(solution)/shard_map/reduce_scatter | solution.py:124
  279.6 1.2 fusion.29
  280.9 2.0 fusion.30
  (115 shorter events, 12.8 us)
Async XLA Ops:
  6.5 29.9 %copy-start = (bf16[2048,256]{1,0:T(8,128)(2,1)S(1)}, bf16[2048,256]{1,0:T(8,128)(2,1)}, u32[]{:S(2)}) copy-start(bf16[2048,256]{1,0:T(8,128)(2,1)} %param.14) | copy-start | bytes 3145732
  6.5 27.7 %all-gather.2.cloned.1.call-start = ((), (), s32[]{:S(2)}) async-start(), calls=%async_computation.3 | async-start | bytes 2621440 | tf_op jit(solution)/shard_map/all_gather | solution.py:84
  7.3 31.6 %copy-start.6 = (bf16[2048,256]{1,0:T(8,128)(2,1)S(1)}, bf16[2048,256]{1,0:T(8,128)(2,1)}, u32[]{:S(2)}) copy-start(bf16[2048,256]{1,0:T(8,128)(2,1)} %param.15) | copy-start | bytes 3145732
  7.3 31.6 %copy-start.7 = (f32[2048]{0:T(1024)S(1)}, f32[2048]{0:T(1024)}, u32[]{:S(2)}) copy-start(f32[2048]{0:T(1024)} %param.12) | copy-start | bytes 24580
  34.2 4.6 %copy-start.1 = (bf16[8,64,2048]{2,1,0:T(8,128)(2,1)S(1)}, bf16[8,64,2048]{2,1,0:T(8,128)(2,1)}, u32[]{:S(2)}) copy-start(bf16[8,64,2048]{2,1,0:T(8,128)(2,1)} %all-gather.2.cloned.1.call-done) | copy-start | bytes 6291460
  38.8 2.2 copy-start.4
  46.1 5.9 %copy-start.8 = (f32[8]{0:T(128)S(1)}, f32[8]{0:T(128)}, u32[]{:S(2)}) copy-start(f32[8]{0:T(128)} %param.16) | copy-start | bytes 100
  46.1 76.9 %all-to-all-start = ((bf16[64,64,384]{2,1,0:T(8,128)(2,1)}), bf16[64,64,384]{2,1,0:T(8,128)(2,1)}, u32[]{:S(2)}, u32[]{:S(2)}) async-start(bf16[64,64,384]{2,1,0:T(8,128)(2,1)} %pad_maximum_fusion), calls=%async_computation | async-start | bytes 6291456 | tf_op jit(solution)/shard_map/all_to_all | solution.py:95
  51.7 227.9 %reduce-scatter.2.cloned.1.call-start = ((), (), s32[]{:S(2)}) async-start(), calls=%async_computation.4 | async-start | bytes 2621440 | tf_op jit(solution)/shard_map/reduce_scatter | solution.py:124
  127.5 2.8 copy-start.2
  135.3 3.2 %copy-start.3 = (bf16[8,512,128]{2,1,0:T(8,128)(2,1)S(1)}, bf16[8,512,128]{2,1,0:T(8,128)(2,1)}, u32[]{:S(2)}) copy-start(bf16[8,512,128]{2,1,0:T(8,128)(2,1)} %copy-done.2) | copy-start | bytes 3145732 | tf_op jit(solution)/shard_map/while
  138.4 2.8 copy-start.2
  146.2 3.2 %copy-start.3 = (bf16[8,512,128]{2,1,0:T(8,128)(2,1)S(1)}, bf16[8,512,128]{2,1,0:T(8,128)(2,1)}, u32[]{:S(2)}) copy-start(bf16[8,512,128]{2,1,0:T(8,128)(2,1)} %copy-done.2) | copy-start | bytes 3145732 | tf_op jit(solution)/shard_map/while
  149.4 2.8 copy-start.2
  157.1 3.2 %copy-start.3 = (bf16[8,512,128]{2,1,0:T(8,128)(2,1)S(1)}, bf16[8,512,128]{2,1,0:T(8,128)(2,1)}, u32[]{:S(2)}) copy-start(bf16[8,512,128]{2,1,0:T(8,128)(2,1)} %copy-done.2) | copy-start | bytes 3145732 | tf_op jit(solution)/shard_map/while
  160.3 2.8 copy-start.2
  168.1 3.2 %copy-start.3 = (bf16[8,512,128]{2,1,0:T(8,128)(2,1)S(1)}, bf16[8,512,128]{2,1,0:T(8,128)(2,1)}, u32[]{:S(2)}) copy-start(bf16[8,512,128]{2,1,0:T(8,128)(2,1)} %copy-done.2) | copy-start | bytes 3145732 | tf_op jit(solution)/shard_map/while
  171.3 2.8 copy-start.2
  179.0 3.2 %copy-start.3 = (bf16[8,512,128]{2,1,0:T(8,128)(2,1)S(1)}, bf16[8,512,128]{2,1,0:T(8,128)(2,1)}, u32[]{:S(2)}) copy-start(bf16[8,512,128]{2,1,0:T(8,128)(2,1)} %copy-done.2) | copy-start | bytes 3145732 | tf_op jit(solution)/shard_map/while
  182.2 2.8 copy-start.2
  190.0 3.2 %copy-start.3 = (bf16[8,512,128]{2,1,0:T(8,128)(2,1)S(1)}, bf16[8,512,128]{2,1,0:T(8,128)(2,1)}, u32[]{:S(2)}) copy-start(bf16[8,512,128]{2,1,0:T(8,128)(2,1)} %copy-done.2) | copy-start | bytes 3145732 | tf_op jit(solution)/shard_map/while
  193.2 2.8 copy-start.2
  200.9 3.2 %copy-start.3 = (bf16[8,512,128]{2,1,0:T(8,128)(2,1)S(1)}, bf16[8,512,128]{2,1,0:T(8,128)(2,1)}, u32[]{:S(2)}) copy-start(bf16[8,512,128]{2,1,0:T(8,128)(2,1)} %copy-done.2) | copy-start | bytes 3145732 | tf_op jit(solution)/shard_map/while
  204.1 2.8 copy-start.2
  211.9 3.2 %copy-start.3 = (bf16[8,512,128]{2,1,0:T(8,128)(2,1)S(1)}, bf16[8,512,128]{2,1,0:T(8,128)(2,1)}, u32[]{:S(2)}) copy-start(bf16[8,512,128]{2,1,0:T(8,128)(2,1)} %copy-done.2) | copy-start | bytes 3145732 | tf_op jit(solution)/shard_map/while
  215.1 31.5 %copy-start.5 = (bf16[1024,2048]{1,0:T(8,128)(2,1)S(1)}, bf16[1024,2048]{1,0:T(8,128)(2,1)}, u32[]{:S(2)}) copy-start(bf16[1024,2048]{1,0:T(8,128)(2,1)} %param.17) | copy-start | bytes 12582916
Sparse Core Ops, SparseCore 0:
  8.9 25.2 all-gather.1
  250.3 29.2 reduce-scatter.1
where the time goes:
time: 290 us
  waiting for transfers between devices  128 us (44%)
  other arithmetic  54.4 us (19%)
  matrix products  41.3 us (14%)
  blocking collectives  29.3 us (10%)
  local copies, waits for them, and re-layouts  16.9 us (6%)
  between operations  13.5 us (5%)
  starting transfers between devices  5.87 us (2%)
    all_to_all x1, waiting for transfers between devices, local(): lax.all_to_all(combined.reshape(item_count, tok_rows, 3 * HEAD_DIM), 'sp'...  70.8 us
    another operation x16, other arithmetic, query_block(): carried, accumulated = lax.fori_loop(0, block_index + 1, key_block, initial)  38.6 us
    reduce_scatter x1, waiting for transfers between devices, local(): lax.psum_scatter(term_rows.astype(jnp.float32).astype(jnp.bfloat16), 'dp'...  29.4 us
    all_to_all x1, blocking collectives, local(): lax.all_to_all(attended, 'sp', split_axis=1, concat_axis=0, tiled=True)  29.3 us
    all_gather x1, waiting for transfers between devices, local(): lax.all_gather(tokens, 'dp', axis=0, tiled=True)  26.9 us
    dot_general x8, matrix products, key_block(): jnp.einsum('qc,kc->qk', query_rows, key_rows, preferred_element_type=jnp....  16.9 us
    dot_general x8, matrix products, key_block(): jnp.dot(weights, value_rows, preferred_element_type=jnp.float32)  15.3 us
    convert_element_type x8, other arithmetic, key_block(): weights = jnp.where(causal, jnp.exp(jax.nn.log_sigmoid(scores) + after_su...  7.18 us
  transfers between devices with their start and end apart: 3, of which 3 were waited for; matrix products, arithmetic and copies ran while one was open for 0% of the time, Pallas kernels for 0%

commit v1 on v0

--- a/solution.py
+++ b/solution.py
@@ -1,8 +1,11 @@
+import functools
 import math
 
 import jax
 import jax.numpy as jnp
 from jax import lax
+from jax.experimental import pallas as pl
+from jax.experimental.pallas import tpu as pltpu
 from jax.sharding import PartitionSpec as P
 
 HEAD_DIM = 128
@@ -72,7 +75,7 @@
     return blocks.reshape(seq_length, HEAD_DIM)
 
 
-def local(tokens, norm_gain, w_query, w_key, w_value, break_bias, w_out):
+def exchanged(tokens, norm_gain, w_query, w_key, w_value, break_bias, w_out):
     own_seqs = tokens.shape[0]
     seq_count = lax.axis_size("dp") * own_seqs
     seq_parts = lax.axis_size("sp")
@@ -125,6 +128,384 @@
         term_rows.astype(jnp.float32).astype(jnp.bfloat16), "dp", scatter_dimension=0, tiled=True
     ).astype(jnp.float32)
     return normalize(summed).astype(jnp.bfloat16)
+
+
+def remote(src, dst, send_sem, recv_sem, sp, dp):
+    return pltpu.make_async_remote_copy(
+        src_ref=src,
+        dst_ref=dst,
+        send_sem=send_sem,
+        recv_sem=recv_sem,
+        device_id={"sp": sp, "dp": dp},
+        device_id_type=pl.DeviceIdType.MESH,
+    )
+
+
+def greet(sp, dp):
+    pl.semaphore_signal(
+        pltpu.get_barrier_semaphore(),
+        inc=1,
+        device_id={"sp": sp, "dp": dp},
+        device_id_type=pl.DeviceIdType.MESH,
+    )
+
+
+def loop(count, body):
+    lax.fori_loop(0, count, lambda step, carry: (body(step), carry)[1], 0)
+
+
+def gather_kernel(sp_count, dp_count, x_ref, out_ref, send_a, recv_a, send_x, recv_x, send_p, recv_p):
+    my_sp, my_dp = lax.axis_index("sp"), lax.axis_index("dp")
+    own, _, part, _ = x_ref.shape
+    pairs = dp_count // 2
+    my_x, my_core = my_dp // 2, lax.rem(my_dp, 2)
+    other = my_x * 2 + 1 - my_core
+    at_home = my_sp // own == my_dp
+
+    def greet_source(step):
+        @pl.when(jnp.logical_not(jnp.logical_and(at_home, step == my_sp)))
+        def _():
+            greet(step, my_sp // own)
+
+    loop(sp_count, greet_source)
+    for step in range(1, dp_count):
+        greet(my_sp, lax.rem(my_dp + step, dp_count))
+    pl.semaphore_wait(
+        pltpu.get_barrier_semaphore(), sp_count + dp_count - 1 - at_home.astype(jnp.int32)
+    )
+
+    def first_copy(s, q):
+        return remote(
+            x_ref.at[s, q], out_ref.at[my_sp, q], send_a.at[s, q], recv_a.at[my_sp], my_dp * own + s, q
+        )
+
+    def is_self(s, q):
+        return jnp.logical_and(my_dp * own + s == my_sp, q == my_dp)
+
+    for s in range(own):
+        for q in range(dp_count):
+
+            @pl.when(jnp.logical_not(is_self(s, q)))
+            def _():
+                first_copy(s, q).start()
+
+            @pl.when(is_self(s, q))
+            def _():
+                pltpu.make_async_copy(
+                    x_ref.at[s, q], out_ref.at[my_sp, q], recv_a.at[my_sp]
+                ).start()
+
+    def across(j, step):
+        block = out_ref.at[j, my_dp]
+        target = lax.rem(my_x + step, pairs) * 2 + my_core
+        return remote(block, block, send_x.at[step - 1, j], recv_x.at[step - 1, j], my_sp, target)
+
+    def inside(j, x):
+        block = out_ref.at[j, x * 2 + my_core]
+        return remote(block, block, send_p.at[x, j], recv_p.at[x, j], my_sp, other)
+
+    def arrived(j, q, sem):
+        block = out_ref.at[j, q]
+        pltpu.make_async_copy(block, block, sem).wait()
+
+    def hand_on(step):
+        j = lax.rem(my_sp + step, sp_count)
+        arrived(j, my_dp, recv_a.at[j])
+        for hop in range(1, pairs):
+            across(j, hop).start()
+        inside(j, my_x).start()
+
+    loop(sp_count, hand_on)
+
+    def relay(step):
+        j = lax.rem(my_sp + step, sp_count)
+        for hop in range(1, pairs):
+            x = lax.rem(my_x - hop + pairs, pairs)
+            arrived(j, x * 2 + my_core, recv_x.at[hop - 1, j])
+            inside(j, x).start()
+
+    loop(sp_count, relay)
+
+    def finish(j):
+        for x in range(pairs):
+            arrived(j, x * 2 + 1 - my_core, recv_p.at[x, j])
+            inside(j, x).wait_send()
+        for hop in range(1, pairs):
+            across(j, hop).wait_send()
+
+    loop(sp_count, finish)
+    for s in range(own):
+        for q in range(dp_count):
+
+            @pl.when(jnp.logical_not(is_self(s, q)))
+            def _():
+                first_copy(s, q).wait_send()
+
+
+def gather_sequence(blocks, sp_count):
+    own, dp_count, part, width = blocks.shape
+    pairs = dp_count // 2
+    return pl.pallas_call(
+        functools.partial(gather_kernel, sp_count, dp_count),
+        out_shape=jax.ShapeDtypeStruct((sp_count, dp_count, part, width), blocks.dtype),
+        in_specs=[pl.BlockSpec(memory_space=pltpu.VMEM)],
+        out_specs=pl.BlockSpec(memory_space=pltpu.VMEM),
+        scratch_shapes=[
+            pltpu.SemaphoreType.DMA((own, dp_count)),
+            pltpu.SemaphoreType.DMA((sp_count,)),
+            pltpu.SemaphoreType.DMA((pairs - 1, sp_count)),
+            pltpu.SemaphoreType.DMA((pairs - 1, sp_count)),
+            pltpu.SemaphoreType.DMA((pairs, sp_count)),
+            pltpu.SemaphoreType.DMA((pairs, sp_count)),
+        ],
+        compiler_params=pltpu.CompilerParams(collective_id=1, has_side_effects=True),
+        name="gather_sequence",
+    )(blocks)
+
+
+def attention_kernel(block, bias_ref, q_ref, k_ref, v_ref, o_ref):
+    length = q_ref.shape[0]
+    log2e = math.log2(math.e)
+    bias = bias_ref[pl.program_id(0)] * log2e
+    scale = HEAD_DIM ** (-0.5) * log2e
+    row = lax.broadcasted_iota(jnp.int32, (2 * block, 2 * block), 0)
+    col = lax.broadcasted_iota(jnp.int32, (2 * block, 2 * block), 1)
+    row = jnp.where(row >= block, row - block, row)
+    summing = jnp.where(jnp.logical_or(col >= block, row > col), 1.0, 0.0).astype(jnp.bfloat16)
+    at_row = lax.broadcasted_iota(jnp.int32, (block, block), 0)
+    at_col = lax.broadcasted_iota(jnp.int32, (block, block), 1)
+    causal = at_col < at_row
+    for r in range(length // block):
+        rows = pl.ds(r * block, block)
+        query = q_ref[rows, :]
+        carried = None
+        total = None
+        for c in range(r, -1, -1):
+            keys = pl.ds(c * block, block)
+            scores = (
+                lax.dot_general(
+                    query,
+                    k_ref[keys, :],
+                    (((1,), (1,)), ((), ())),
+                    preferred_element_type=jnp.float32,
+                )
+                * scale
+                + bias
+            )
+            soft = jnp.log2(1.0 + jnp.exp2(-jnp.abs(scores)))
+            log_keep = -jnp.maximum(scores, 0.0) - soft
+            log_break = jnp.minimum(scores, 0.0) - soft
+            if c == r:
+                log_keep = jnp.where(causal, log_keep, 0.0)
+            high = log_keep.astype(jnp.bfloat16)
+            low = (log_keep - high.astype(jnp.float32)).astype(jnp.bfloat16)
+            sums = jnp.dot(
+                jnp.concatenate((high, low), axis=1), summing, preferred_element_type=jnp.float32
+            )
+            exponent = log_break + sums[:, :block]
+            if carried is not None:
+                exponent = exponent + carried
+            weights = jnp.exp2(exponent)
+            if c == r:
+                weights = jnp.where(causal, weights, 0.0)
+            term = jnp.dot(
+                weights.astype(jnp.bfloat16), v_ref[keys, :], preferred_element_type=jnp.float32
+            )
+            carried = sums[:, block:] if carried is None else carried + sums[:, block:]
+            total = term if total is None else total + term
+        o_ref[rows, :] = total.astype(jnp.bfloat16)
+
+
+def attention(query, keys, values, bias, copies):
+    length, columns = query.shape
+    heads = columns // HEAD_DIM
+    block = math.gcd(length, 128)
+    return pl.pallas_call(
+        functools.partial(attention_kernel, block),
+        grid=(heads,),
+        out_shape=jax.ShapeDtypeStruct((length, columns), jnp.bfloat16),
+        in_specs=[
+            pl.BlockSpec(memory_space=pltpu.SMEM),
+            pl.BlockSpec((length, HEAD_DIM), lambda h: (0, h)),
+            pl.BlockSpec((length, HEAD_DIM), lambda h: (0, h // copies)),
+            pl.BlockSpec((length, HEAD_DIM), lambda h: (0, h // copies)),
+        ],
+        out_specs=pl.BlockSpec((length, HEAD_DIM), lambda h: (0, h)),
+        name="attention",
+    )(bias, query, keys, values)
+
+
+def return_kernel(
+    sp_count, dp_count, own, p_ref, out_ref, from_core, summed, from_x, done,
+    send_p, recv_p, send_x, recv_x, send_h, recv_h,
+):
+    my_sp, my_dp = lax.axis_index("sp"), lax.axis_index("dp")
+    pairs = dp_count // 2
+    my_x, my_core = my_dp // 2, lax.rem(my_dp, 2)
+    other = my_x * 2 + 1 - my_core
+    home_dp = my_sp // own
+    at_home = home_dp == my_dp
+
+    def greet_source(step):
+        s, q = step // dp_count, lax.rem(step, dp_count)
+
+        @pl.when(jnp.logical_not(jnp.logical_and(my_dp * own + s == my_sp, q == my_dp)))
+        def _():
+            greet(my_dp * own + s, q)
+
+    loop(own * dp_count, greet_source)
+    for step in range(1, dp_count):
+        greet(my_sp, lax.rem(my_dp + step, dp_count))
+    pl.semaphore_wait(
+        pltpu.get_barrier_semaphore(), sp_count + dp_count - 1 - at_home.astype(jnp.int32)
+    )
+
+    def inside(j, hop):
+        x = lax.rem(my_x + hop, pairs)
+        return remote(
+            p_ref.at[j, x * 2 + 1 - my_core],
+            from_core.at[hop, j],
+            send_p.at[hop, j],
+            recv_p.at[hop, j],
+            my_sp,
+            other,
+        )
+
+    def across(j, hop):
+        x = lax.rem(my_x + hop, pairs)
+        return remote(
+            summed.at[hop - 1, j],
+            from_x.at[hop - 1, j],
+            send_x.at[hop - 1, j],
+            recv_x.at[hop - 1, j],
+            my_sp,
+            x * 2 + my_core,
+        )
+
+    def homeward(j):
+        return remote(
+            done.at[j],
+            out_ref.at[lax.rem(my_sp, own), my_dp],
+            send_h.at[j],
+            recv_h.at[lax.rem(my_sp, own), my_dp],
+            j,
+            home_dp,
+        )
+
+    hops = list(range(1, pairs)) + [0]
+    for hop in hops:
+        loop(sp_count, lambda j: inside(j, hop).start())
+
+    def send_sums(step):
+        j = lax.rem(my_sp + step, sp_count)
+        for hop in range(1, pairs):
+            inside(j, hop).wait_recv()
+            mine = p_ref[j, lax.rem(my_x + hop, pairs) * 2 + my_core].astype(jnp.float32)
+            summed[hop - 1, j] = (mine + from_core[hop, j].astype(jnp.float32)).astype(jnp.bfloat16)
+            across(j, hop).start()
+
+    loop(sp_count, send_sums)
+
+    def is_self(j):
+        return jnp.logical_and(at_home, j == my_sp)
+
+    def complete(step):
+        j = lax.rem(my_sp + step, sp_count)
+        inside(j, 0).wait_recv()
+        total = p_ref[j, my_dp].astype(jnp.float32) + from_core[0, j].astype(jnp.float32)
+        for hop in range(1, pairs):
+            across(j, hop).wait_recv()
+            total = total + from_x[hop - 1, j].astype(jnp.float32)
+        done[j] = normalize(total).astype(jnp.bfloat16)
+
+        @pl.when(jnp.logical_not(is_self(j)))
+        def _():
+            homeward(j).start()
+
+        @pl.when(is_self(j))
+        def _():
+            pltpu.make_async_copy(
+                done.at[j],
+                out_ref.at[lax.rem(my_sp, own), my_dp],
+                recv_h.at[lax.rem(my_sp, own), my_dp],
+            ).start()
+
+    loop(sp_count, complete)
+
+    def finish(j):
+        for hop in range(pairs):
+            inside(j, hop).wait_send()
+        for hop in range(1, pairs):
+            across(j, hop).wait_send()
+
+        @pl.when(jnp.logical_not(is_self(j)))
+        def _():
+            homeward(j).wait_send()
+
+    loop(sp_count, finish)
+    for s in range(own):
+        for q in range(dp_count):
+            block = out_ref.at[s, q]
+            pltpu.make_async_copy(block, block, recv_h.at[s, q]).wait()
+
+
+def return_home(partial, own):
+    sp_count, dp_count, part, width = partial.shape
+    pairs = dp_count // 2
+    rows = (sp_count, part, width)
+    return pl.pallas_call(
+        functools.partial(return_kernel, sp_count, dp_count, own),
+        out_shape=jax.ShapeDtypeStruct((own, dp_count, part, width), jnp.bfloat16),
+        in_specs=[pl.BlockSpec(memory_space=pltpu.VMEM)],
+        out_specs=pl.BlockSpec(memory_space=pltpu.VMEM),
+        scratch_shapes=[
+            pltpu.VMEM((pairs, *rows), jnp.bfloat16),
+            pltpu.VMEM((pairs - 1, *rows), jnp.bfloat16),
+            pltpu.VMEM((pairs - 1, *rows), jnp.bfloat16),
+            pltpu.VMEM(rows, jnp.bfloat16),
+            pltpu.SemaphoreType.DMA((pairs, sp_count)),
+            pltpu.SemaphoreType.DMA((pairs, sp_count)),
+            pltpu.SemaphoreType.DMA((pairs - 1, sp_count)),
+            pltpu.SemaphoreType.DMA((pairs - 1, sp_count)),
+            pltpu.SemaphoreType.DMA((sp_count,)),
+            pltpu.SemaphoreType.DMA((own, dp_count)),
+        ],
+        compiler_params=pltpu.CompilerParams(collective_id=2, has_side_effects=True),
+        name="return_home",
+    )(partial)
+
+
+def gathered(tokens, norm_gain, w_query, w_key, w_value, break_bias, w_out):
+    own, tok_rows, width = tokens.shape
+    sp_count, dp_count = lax.axis_size("sp"), lax.axis_size("dp")
+    normed = (normalize(tokens) * norm_gain).astype(jnp.bfloat16)
+    rows = gather_sequence(
+        normed.reshape(own, dp_count, tok_rows // dp_count, width), sp_count
+    ).reshape(sp_count * tok_rows, width)
+
+    def project(weight):
+        return jnp.dot(rows, weight, preferred_element_type=jnp.float32).astype(jnp.bfloat16)
+
+    attended = attention(
+        project(w_query),
+        project(w_key),
+        project(w_value),
+        break_bias,
+        w_query.shape[1] // w_key.shape[1],
+    )
+    partial = jnp.dot(attended, w_out, preferred_element_type=jnp.float32).astype(jnp.bfloat16)
+    mixed = return_home(
+        partial.reshape(sp_count, dp_count, tok_rows // dp_count, width), own
+    )
+    return mixed.reshape(own, tok_rows, width)
+
+
+def local(tokens, *rest):
+    sp_count, dp_count = lax.axis_size("sp"), lax.axis_size("dp")
+    one_each = dp_count * tokens.shape[0] == sp_count
+    if one_each and dp_count % 2 == 0 and dp_count > 2 and tokens.shape[1] % (16 * dp_count) == 0:
+        return gathered(tokens, *rest)
+    return exchanged(tokens, *rest)
 
 
 def solution(mesh):

time: 290 us -> 107 us (0.37)
  waiting for transfers between devices: 128 us -> 0 us
  Pallas kernels: 0 us -> 87.3 us
  other arithmetic: 54.4 us -> 3.36 us
  blocking collectives: 29.3 us -> 0 us
  matrix products: 41.3 us -> 14.1 us
  local copies, waits for them, and re-layouts: 16.9 us -> 1.9 us
  between operations: 13.5 us -> 0.05 us
  starting transfers between devices: 5.87 us -> 0 us
    pallas_call x0 -> x3, Pallas kernels: none -> 87.3 us  [the longest x1 36.9 us: return_home(): pl.pallas_call(functools.partial(return_kernel, sp_count, dp_count, own),...]
    all_to_all x1 -> x0, waiting for transfers between devices: 70.8 us -> none  [local(): lax.all_to_all(combined.reshape(item_count, tok_rows, 3 * HEAD_DIM), 'sp'...]
    another operation x24 -> x0, other arithmetic: 39.4 us -> none  [the longest x16 38.6 us: query_block(): carried, accumulated = lax.fori_loop(0, block_index + 1, key_block, initial)]
    reduce_scatter x1 -> x0, waiting for transfers between devices: 29.4 us -> none  [local(): lax.psum_scatter(term_rows.astype(jnp.float32).astype(jnp.bfloat16), 'dp'...]
    all_to_all x1 -> x0, blocking collectives: 29.3 us -> none  [local(): lax.all_to_all(attended, 'sp', split_axis=1, concat_axis=0, tiled=True)]
    dot_general x20 -> x4, matrix products: 41.3 us -> 14.1 us  [the longest x3 7.91 us: project(): jnp.dot(rows, weight, preferred_element_type=jnp.float32)]
    all_gather x1 -> x0, waiting for transfers between devices: 26.9 us -> none  [local(): lax.all_gather(tokens, 'dp', axis=0, tiled=True)]
    convert_element_type x9 -> x1, other arithmetic: 9.17 us -> 2.03 us  [gathered(): normed = (normalize(tokens) * norm_gain).astype(jnp.bfloat16)]
  transfers between devices with their start and end apart: 3 -> 0, of which waited for: 3 -> 0; matrix products, arithmetic and copies ran while one was open for 0% -> 0% of each run, Pallas kernels for 0% -> 0%
where the time goes in v1:
time: 107 us
  Pallas kernels  87.3 us (82%)
  matrix products  14.1 us (13%)
  other arithmetic  3.36 us (3%)
  local copies, waits for them, and re-layouts  1.9 us (2%)
    pallas_call x1, Pallas kernels, return_home(): pl.pallas_call(functools.partial(return_kernel, sp_count, dp_count, own),...  36.9 us
    pallas_call x1, Pallas kernels, gather_sequence(): pl.pallas_call(functools.partial(gather_kernel, sp_count, dp_count), out_...  35.4 us
    pallas_call x1, Pallas kernels, attention(): pl.pallas_call(functools.partial(attention_kernel, block), grid=(heads,),...  15 us
    dot_general x3, matrix products, project(): jnp.dot(rows, weight, preferred_element_type=jnp.float32)  7.91 us
    dot_general x1, matrix products, gathered(): jnp.dot(attended, w_out, preferred_element_type=jnp.float32)  6.19 us

profile of v1, /device:TPU:0, one launch (start us, length us, event | category | flops | bytes accessed | tf_op | source)
XLA Modules:
  0.0 106.7 jit_solution(17303082497647126544)
XLA Ops:
  0.0 0.0 copy-start
  0.0 1.3 %fusion = f32[2,64]{1,0:T(2,128)S(1)} fusion(bf16[2,64,2048]{2,1,0:T(8,128)(2,1)} %param.7), kind=kLoop, calls=%fused_computation.6 | loop fusion | flops 786304 | bytes 524800 | tf_op jit(solution)/shard_map/reduce_sum | solution.py:19
  1.3 2.0 %fusion.2 = bf16[2,64,2048]{2,1,0:T(8,128)(2,1)} fusion(bf16[2,64,2048]{2,1,0:T(8,128)(2,1)} %param.7, f32[2048]{0:T(1024)} %param.8, f32[2,64]{1,0:T(2,128)S(1)} %add_rsqrt_fusion), kind=kLoop, calls=%fused_computation.8 | loop fusion | flops 1048576 | bytes 1057280 | tf_op jit(solution)/shard_map/convert_element_type | solution.py:481
  3.4 35.4 %gather_sequence.1 = bf16[8,4,16,2048]{3,2,1,0:T(8,128)(2,1)} custom-call(bf16[2,4,16,2048]{3,2,1,0:T(8,128)(2,1)} %bitcast.12), custom_call_target="tpu_custom_call" | custom-call | tf_op jit(solution)/shard_map/gather_sequence/pallas_call | solution.py:248
  38.8 0.0 copy-start.1
  38.8 0.0 copy-start.3
  38.8 0.0 copy-done
  38.8 0.0 copy-start.2
  38.8 3.2 %convolution_convert_fusion.2.v_ref = bf16[512,256]{1,0:T(8,128)(2,1)} fusion(bf16[512,2048]{1,0:T(8,128)(2,1)} %bitcast.13, bf16[2048,256]{1,0:T(8,128)(2,1)S(1)} %copy-done), kind=kOutput, calls=%fused_computation.4 | convolution fusion | flops 537001984 | bytes 3407872 | tf_op jit(solution)/shard_map/dot_general | solution.py:487
  42.0 0.0 copy-done.1
  42.0 0.0 copy-done.3
  42.0 1.4 %convolution_convert_fusion.3.k_ref = bf16[512,256]{1,0:T(8,128)(2,1)} fusion(bf16[512,2048]{1,0:T(8,128)(2,1)S(1)} %bitcast.14, bf16[2048,256]{1,0:T(8,128)(2,1)S(1)} %copy-done.3), kind=kOutput, calls=%fused_computation.5 | convolution fusion | flops 537001984 | bytes 3407872 | tf_op jit(solution)/shard_map/dot_general | solution.py:487
  43.4 0.0 copy-done.2
  43.4 3.3 %convolution_convert_fusion.1.q_ref = bf16[512,1024]{1,0:T(8,128)(2,1)} fusion(bf16[512,2048]{1,0:T(8,128)(2,1)S(1)} %bitcast.15, bf16[2048,1024]{1,0:T(8,128)(2,1)S(1)} %copy-done.2), kind=kOutput, calls=%fused_computation.1 | convolution fusion | flops 2148007936 | bytes 7340032 | tf_op jit(solution)/shard_map/dot_general | solution.py:487
  46.8 15.0 %attention.1 = bf16[512,1024]{1,0:T(8,128)(2,1)} custom-call(f32[8]{0:T(128)} %bias_ref.1, bf16[512,1024]{1,0:T(8,128)(2,1)} %convolution_convert_fusion.1.q_ref, bf16[512,256]{1,0:T(8,128)(2,1)} %convolution_convert_fusion.3.k_ref, bf16[512,256]{1,0:T(8,128)(2,1)} %convolution_convert_fusion.2.v_ref), custom_call_target="tpu_custom_call" | custom-call | tf_op jit(solution)/shard_map/attention/pallas_call | solution.py:323
  61.8 6.2 %convolution_convert_fusion = bf16[512,2048]{1,0:T(8,128)(2,1)} fusion(bf16[512,1024]{1,0:T(8,128)(2,1)} %attention.1, bf16[1024,2048]{1,0:T(8,128)(2,1)} %param.13), kind=kOutput, calls=%fused_computation | convolution fusion | flops 2148532224 | bytes 7340032 | tf_op jit(solution)/shard_map/dot_general | solution.py:496
  68.0 36.9 %return_home.1 = bf16[2,4,16,2048]{3,2,1,0:T(8,128)(2,1)} custom-call(bf16[8,4,16,2048]{3,2,1,0:T(8,128)(2,1)} %bitcast.16), custom_call_target="tpu_custom_call" | custom-call | tf_op jit(solution)/shard_map/return_home/pallas_call | solution.py:456
  104.9 1.9 %copy.9 = bf16[2,64,2048]{2,1,0:T(8,128)(2,1)} copy(bf16[2,64,2048]{2,1,0:T(8,128)(2,1)} %bitcast.17) | data formatting | bytes 1048576
  (1 shorter events, 0.0 us)
Async XLA Ops:
  0.0 38.8 %copy-start = (bf16[2048,256]{1,0:T(8,128)(2,1)S(1)}, bf16[2048,256]{1,0:T(8,128)(2,1)}, u32[]{:S(2)}) copy-start(bf16[2048,256]{1,0:T(8,128)(2,1)} %param.11) | copy-start | bytes 3145732
  38.8 3.2 %copy-start.1 = (bf16[8,4,16,2048]{3,2,1,0:T(8,128)(2,1)S(1)}, bf16[8,4,16,2048]{3,2,1,0:T(8,128)(2,1)}, u32[]{:S(2)}) copy-start(bf16[8,4,16,2048]{3,2,1,0:T(8,128)(2,1)} %gather_sequence.1) | copy-start | bytes 6291460
  38.8 3.2 %copy-start.3 = (bf16[2048,256]{1,0:T(8,128)(2,1)S(1)}, bf16[2048,256]{1,0:T(8,128)(2,1)}, u32[]{:S(2)}) copy-start(bf16[2048,256]{1,0:T(8,128)(2,1)} %param.10) | copy-start | bytes 3145732
  38.8 4.6 %copy-start.2 = (bf16[2048,1024]{1,0:T(8,128)(2,1)S(1)}, bf16[2048,1024]{1,0:T(8,128)(2,1)}, u32[]{:S(2)}) copy-start(bf16[2048,1024]{1,0:T(8,128)(2,1)} %param.9) | copy-start | bytes 12582916

commit v2 on v0

--- a/solution.py
+++ b/solution.py
@@ -1,8 +1,11 @@
+import functools
 import math
 
 import jax
 import jax.numpy as jnp
 from jax import lax
+from jax.experimental import pallas as pl
+from jax.experimental.pallas import tpu as pltpu
 from jax.sharding import PartitionSpec as P
 
 HEAD_DIM = 128
@@ -72,7 +75,7 @@
     return blocks.reshape(seq_length, HEAD_DIM)
 
 
-def local(tokens, norm_gain, w_query, w_key, w_value, break_bias, w_out):
+def exchanged(tokens, norm_gain, w_query, w_key, w_value, break_bias, w_out):
     own_seqs = tokens.shape[0]
     seq_count = lax.axis_size("dp") * own_seqs
     seq_parts = lax.axis_size("sp")
@@ -125,6 +128,412 @@
         term_rows.astype(jnp.float32).astype(jnp.bfloat16), "dp", scatter_dimension=0, tiled=True
     ).astype(jnp.float32)
     return normalize(summed).astype(jnp.bfloat16)
+
+
+def remote(src, dst, send_sem, recv_sem, sp, dp):
+    return pltpu.make_async_remote_copy(
+        src_ref=src,
+        dst_ref=dst,
+        send_sem=send_sem,
+        recv_sem=recv_sem,
+        device_id={"sp": sp, "dp": dp},
+        device_id_type=pl.DeviceIdType.MESH,
+    )
+
+
+def greet(sp, dp):
+    pl.semaphore_signal(
+        pltpu.get_barrier_semaphore(),
+        inc=1,
+        device_id={"sp": sp, "dp": dp},
+        device_id_type=pl.DeviceIdType.MESH,
+    )
+
+
+def loop(count, body):
+    lax.fori_loop(0, count, lambda step, carry: (body(step), carry)[1], 0)
+
+
+def layer_kernel(
+    sp_count, dp_count, copies, block, x_ref, gain_ref, bias_ref, wq_hbm, wk_hbm, wv_hbm, wo_hbm, out_ref,
+    wq, wk, wv, wo, normed, staged, rows_ref, q_ref, k_ref, v_ref, att_ref, p_ref, from_core, summed,
+    from_x, done, home, load_sem, send_1, recv_1, send_2, recv_2, send_x, recv_x, send_p, recv_p,
+    send_c, recv_c, send_s, recv_s, send_3, recv_3, send_4, recv_4,
+):
+    my_sp, my_dp = lax.axis_index("sp"), lax.axis_index("dp")
+    own, _, part, width = x_ref.shape
+    pairs = dp_count // 2
+    my_x, my_core = my_dp // 2, lax.rem(my_dp, 2)
+    other = my_x * 2 + 1 - my_core
+    length = sp_count * dp_count * part
+
+    def at_hop(hop):
+        return lax.rem(my_x + hop, pairs)
+
+    def peer(step):
+        hop, flip = step // 2, step % 2
+        return at_hop(hop) * 2 + (1 - my_core if flip else my_core)
+
+    loop(sp_count - 1, lambda step: greet(lax.rem(my_sp + step + 1, sp_count), my_dp))
+    for step in range(1, dp_count):
+        greet(my_sp, lax.rem(my_dp + step, dp_count))
+
+    loads = [
+        pltpu.make_async_copy(source, target, load_sem.at[place])
+        for place, (source, target) in enumerate(
+            ((wq_hbm, wq), (wk_hbm, wk), (wv_hbm, wv), (wo_hbm, wo))
+        )
+    ]
+    for load in loads:
+        load.start()
+
+    for s in range(own):
+        for q in range(dp_count):
+            normed[q, s] = (normalize(x_ref[s, q]) * gain_ref[...]).astype(jnp.bfloat16)
+    staged[my_dp] = normed[my_dp]
+    pl.semaphore_wait(pltpu.get_barrier_semaphore(), sp_count + dp_count - 2)
+
+    def over_dp(step):
+        q = peer(step)
+        return remote(
+            normed.at[q], staged.at[my_dp], send_1.at[step], recv_1.at[my_dp], my_sp, q
+        )
+
+    def arrived(ref, sem):
+        pltpu.make_async_copy(ref, ref, sem).wait()
+
+    order = list(range(2, dp_count)) + [1]
+    for step in order:
+        over_dp(step).start()
+
+    def over_sp(e, s):
+        i = e * own + s
+        return remote(
+            staged.at[e, s], rows_ref.at[my_sp, my_dp], send_2.at[i], recv_2.at[my_sp], i, my_dp
+        )
+
+    for step in [0, 1] + list(range(2, dp_count)):
+        e = peer(step)
+        if step:
+            arrived(staged.at[e], recv_1.at[e])
+        for s in range(own):
+
+            @pl.when(e * own + s != my_sp)
+            def _():
+                over_sp(e, s).start()
+
+            @pl.when(e * own + s == my_sp)
+            def _():
+                pltpu.make_async_copy(
+                    staged.at[e, s], rows_ref.at[my_sp, my_dp], recv_2.at[my_sp]
+                ).start()
+
+    def across(j, hop):
+        piece = rows_ref.at[j, my_dp]
+        return remote(
+            piece, piece, send_x.at[hop - 1, j], recv_x.at[hop - 1, j], my_sp, at_hop(hop) * 2 + my_core
+        )
+
+    def inside(j, x):
+        piece = rows_ref.at[j, x * 2 + my_core]
+        return remote(piece, piece, send_p.at[x, j], recv_p.at[x, j], my_sp, other)
+
+    def hand_on(step):
+        j = lax.rem(my_sp + step, sp_count)
+        arrived(rows_ref.at[j, my_dp], recv_2.at[j])
+        for hop in range(1, pairs):
+            across(j, hop).start()
+        inside(j, my_x).start()
+
+    loop(sp_count, hand_on)
+
+    def relay(step):
+        j = lax.rem(my_sp + step, sp_count)
+        for hop in range(1, pairs):
+            x = at_hop(pairs - hop)
+            arrived(rows_ref.at[j, x * 2 + my_core], recv_x.at[hop - 1, j])
+            inside(j, x).start()
+
+    loop(sp_count, relay)
+
+    def finish_rows(j):
+        for x in range(pairs):
+            arrived(rows_ref.at[j, x * 2 + 1 - my_core], recv_p.at[x, j])
+
+    loop(sp_count, finish_rows)
+    for load in loads:
+        load.wait()
+
+    rows = rows_ref[...].reshape(length, width)
+
+    def project(weight, target):
+        columns = math.gcd(weight.shape[1], 256)
+
+        def tile(n):
+            at = pl.ds(pl.multiple_of(n * columns, columns), columns)
+            target[:, at] = jnp.dot(
+                rows, weight[:, at], preferred_element_type=jnp.float32
+            ).astype(jnp.bfloat16)
+
+        loop(weight.shape[1] // columns, tile)
+
+    project(wk, k_ref)
+    project(wv, v_ref)
+    project(wq, q_ref)
+
+    def head(h):
+        mine = pl.ds(pl.multiple_of(h * HEAD_DIM, HEAD_DIM), HEAD_DIM)
+        shared = pl.ds(pl.multiple_of(h // copies * HEAD_DIM, HEAD_DIM), HEAD_DIM)
+        attend(block, bias_ref[h], q_ref[:, mine], k_ref[:, shared], v_ref[:, shared], att_ref, mine)
+
+    loop(q_ref.shape[1] // HEAD_DIM, head)
+
+    def chip_copy(j, hop):
+        return remote(
+            p_ref.at[j, at_hop(hop) * 2 + 1 - my_core],
+            from_core.at[hop, j],
+            send_c.at[hop, j],
+            recv_c.at[hop, j],
+            my_sp,
+            other,
+        )
+
+    def sum_copy(j, hop):
+        return remote(
+            summed.at[hop - 1, j],
+            from_x.at[hop - 1, j],
+            send_s.at[hop - 1, j],
+            recv_s.at[hop - 1, j],
+            my_sp,
+            at_hop(hop) * 2 + my_core,
+        )
+
+    hops = list(range(1, pairs)) + [0]
+    some = math.gcd(sp_count, 2)
+    group = sp_count // some
+    wide = math.gcd(width, 512)
+    tall = group * dp_count * part
+
+    def send_sums(j):
+        for hop in range(1, pairs):
+            chip_copy(j, hop).wait_recv()
+            mine = p_ref[j, at_hop(hop) * 2 + my_core].astype(jnp.float32)
+            summed[hop - 1, j] = (mine + from_core[hop, j].astype(jnp.float32)).astype(jnp.bfloat16)
+            sum_copy(j, hop).start()
+
+    for r in range(some):
+        heads = att_ref[r * tall : (r + 1) * tall, :]
+
+        def out_tile(n):
+            at = pl.ds(pl.multiple_of(n * wide, wide), wide)
+            value = jnp.dot(heads, wo[:, at], preferred_element_type=jnp.float32)
+            p_ref[r * group : (r + 1) * group, :, :, at] = value.astype(jnp.bfloat16).reshape(
+                group, dp_count, part, wide
+            )
+
+        loop(width // wide, out_tile)
+        for hop in hops:
+            loop(group, lambda j: chip_copy(r * group + j, hop).start())
+        loop(group, lambda j: send_sums(r * group + j))
+
+    def to_sp(j):
+        return remote(done.at[j], home.at[my_sp], send_3.at[j], recv_3.at[my_sp], j, my_dp)
+
+    def complete(j):
+        chip_copy(j, 0).wait_recv()
+        total = p_ref[j, my_dp].astype(jnp.float32) + from_core[0, j].astype(jnp.float32)
+        for hop in range(1, pairs):
+            sum_copy(j, hop).wait_recv()
+            total = total + from_x[hop - 1, j].astype(jnp.float32)
+        done[j] = normalize(total).astype(jnp.bfloat16)
+
+        @pl.when(j != my_sp)
+        def _():
+            to_sp(j).start()
+
+        @pl.when(j == my_sp)
+        def _():
+            pltpu.make_async_copy(done.at[j], home.at[my_sp], recv_3.at[my_sp]).start()
+
+    loop(sp_count, complete)
+
+    def to_dp(i):
+        e, s = i // own, lax.rem(i, own)
+        return remote(
+            home.at[i], out_ref.at[s, my_dp], send_4.at[i], recv_4.at[s, my_dp], my_sp, e
+        )
+
+    def is_mine(i):
+        return i // own == my_dp
+
+    def send_home(i):
+        arrived(home.at[i], recv_3.at[i])
+
+        @pl.when(jnp.logical_not(is_mine(i)))
+        def _():
+            to_dp(i).start()
+
+        @pl.when(is_mine(i))
+        def _():
+            s = lax.rem(i, own)
+            pltpu.make_async_copy(home.at[i], out_ref.at[s, my_dp], recv_4.at[s, my_dp]).start()
+
+    loop(sp_count, send_home)
+    for s in range(own):
+        for q in range(dp_count):
+            arrived(out_ref.at[s, q], recv_4.at[s, q])
+
+    for step in range(1, dp_count):
+        over_dp(step).wait_send()
+
+    def finish(j):
+        for x in range(pairs):
+            inside(j, x).wait_send()
+            chip_copy(j, x).wait_send()
+        for hop in range(1, pairs):
+            across(j, hop).wait_send()
+            sum_copy(j, hop).wait_send()
+
+        @pl.when(j != my_sp)
+        def _():
+            over_sp(j // own, lax.rem(j, own)).wait_send()
+            to_sp(j).wait_send()
+
+        @pl.when(jnp.logical_not(is_mine(j)))
+        def _():
+            to_dp(j).wait_send()
+
+    loop(sp_count, finish)
+
+
+def attend(block, bias, query_data, key_data, value_data, o_ref, columns):
+    length = query_data.shape[0]
+    log2e = math.log2(math.e)
+    bias = bias * log2e
+    scale = HEAD_DIM ** (-0.5) * log2e
+    row = lax.broadcasted_iota(jnp.int32, (2 * block, 2 * block), 0)
+    col = lax.broadcasted_iota(jnp.int32, (2 * block, 2 * block), 1)
+    row = jnp.where(row >= block, row - block, row)
+    summing = jnp.where(jnp.logical_or(col >= block, row > col), 1.0, 0.0).astype(jnp.bfloat16)
+    at_row = lax.broadcasted_iota(jnp.int32, (block, block), 0)
+    at_col = lax.broadcasted_iota(jnp.int32, (block, block), 1)
+    causal = at_col < at_row
+    for r in range(length // block):
+        rows = slice(r * block, (r + 1) * block)
+        query = query_data[rows]
+        carried = None
+        total = None
+        for c in range(r, -1, -1):
+            keys = slice(c * block, (c + 1) * block)
+            scores = (
+                lax.dot_general(
+                    query,
+                    key_data[keys],
+                    (((1,), (1,)), ((), ())),
+                    preferred_element_type=jnp.float32,
+                )
+                * scale
+                + bias
+            )
+            soft = jnp.log2(1.0 + jnp.exp2(-jnp.abs(scores)))
+            log_keep = -jnp.maximum(scores, 0.0) - soft
+            log_break = jnp.minimum(scores, 0.0) - soft
+            if c == r:
+                log_keep = jnp.where(causal, log_keep, 0.0)
+            high = log_keep.astype(jnp.bfloat16)
+            low = (log_keep - high.astype(jnp.float32)).astype(jnp.bfloat16)
+            sums = jnp.dot(
+                jnp.concatenate((high, low), axis=1), summing, preferred_element_type=jnp.float32
+            )
+            exponent = log_break + sums[:, :block]
+            if carried is not None:
+                exponent = exponent + carried
+            weights = jnp.exp2(exponent)
+            if c == r:
+                weights = jnp.where(causal, weights, 0.0)
+            term = jnp.dot(
+                weights.astype(jnp.bfloat16), value_data[keys], preferred_element_type=jnp.float32
+            )
+            carried = sums[:, block:] if carried is None else carried + sums[:, block:]
+            total = term if total is None else total + term
+        o_ref[rows, columns] = total.astype(jnp.bfloat16)
+
+
+def gathered(tokens, norm_gain, w_query, w_key, w_value, break_bias, w_out):
+    own, tok_rows, width = tokens.shape
+    sp_count, dp_count = lax.axis_size("sp"), lax.axis_size("dp")
+    part = tok_rows // dp_count
+    pairs = dp_count // 2
+    length = sp_count * tok_rows
+    copies = w_query.shape[1] // w_key.shape[1]
+    vmem = pl.BlockSpec(memory_space=pltpu.VMEM)
+    hbm = pl.BlockSpec(memory_space=pl.ANY)
+
+    def room(*shape):
+        return pltpu.VMEM(shape, jnp.bfloat16)
+
+    dma = pltpu.SemaphoreType.DMA
+    mixed = pl.pallas_call(
+        functools.partial(layer_kernel, sp_count, dp_count, copies, math.gcd(length, 128)),
+        out_shape=jax.ShapeDtypeStruct((own, dp_count, part, width), jnp.bfloat16),
+        in_specs=[vmem, vmem, pl.BlockSpec(memory_space=pltpu.SMEM), hbm, hbm, hbm, hbm],
+        out_specs=vmem,
+        scratch_shapes=[
+            room(*w_query.shape),
+            room(*w_key.shape),
+            room(*w_value.shape),
+            room(*w_out.shape),
+            room(dp_count, own, part, width),
+            room(dp_count, own, part, width),
+            room(sp_count, dp_count, part, width),
+            room(length, w_query.shape[1]),
+            room(length, w_key.shape[1]),
+            room(length, w_value.shape[1]),
+            room(length, w_query.shape[1]),
+            room(sp_count, dp_count, part, width),
+            room(pairs, sp_count, part, width),
+            room(pairs - 1, sp_count, part, width),
+            room(pairs - 1, sp_count, part, width),
+            room(sp_count, part, width),
+            room(sp_count, part, width),
+            dma((4,)),
+            dma((dp_count,)),
+            dma((dp_count,)),
+            dma((sp_count,)),
+            dma((sp_count,)),
+            dma((pairs - 1, sp_count)),
+            dma((pairs - 1, sp_count)),
+            dma((pairs, sp_count)),
+            dma((pairs, sp_count)),
+            dma((pairs, sp_count)),
+            dma((pairs, sp_count)),
+            dma((pairs - 1, sp_count)),
+            dma((pairs - 1, sp_count)),
+            dma((sp_count,)),
+            dma((sp_count,)),
+            dma((sp_count,)),
+            dma((own, dp_count)),
+        ],
+        compiler_params=pltpu.CompilerParams(collective_id=1, has_side_effects=True),
+        name="layer",
+    )(
+        tokens.reshape(own, dp_count, part, width),
+        norm_gain.reshape(1, width),
+        break_bias,
+        w_query,
+        w_key,
+        w_value,
+        w_out,
+    )
+    return mixed.reshape(own, tok_rows, width)
+
+
+def local(tokens, *rest):
+    sp_count, dp_count = lax.axis_size("sp"), lax.axis_size("dp")
+    one_each = dp_count * tokens.shape[0] == sp_count
+    if one_each and dp_count % 2 == 0 and dp_count > 2 and tokens.shape[1] % (16 * dp_count) == 0:
+        return gathered(tokens, *rest)
+    return exchanged(tokens, *rest)
 
 
 def solution(mesh):

time: 290 us -> 79.5 us (0.27)
  the two profiles are of different devices: /device:TPU:0 before, /device:TPU:29 now
where the time goes in v2:
time: 79.5 us; the launch traced here: 79.4 us
  Pallas kernels  77.5 us (97%)
  local copies, waits for them, and re-layouts  1.88 us (2%)
    pallas_call x1, Pallas kernels, gathered(): pl.pallas_call(functools.partial(layer_kernel, sp_count, dp_count, copies...  77.5 us
    unnamed x1, local copies, waits for them, and re-layouts  1.88 us

profile of v2, /device:TPU:29, one launch (start us, length us, event | category | flops | bytes accessed | tf_op | source)
XLA Modules:
  0.0 79.4 jit_solution(4728324837398741984)
XLA Ops:
  0.0 77.5 %layer.1 = bf16[2,4,16,2048]{3,2,1,0:T(8,128)(2,1)} custom-call(bf16[2,4,16,2048]{3,2,1,0:T(8,128)(2,1)} %bitcast.4, f32[1,2048]{1,0:T(1,128)} %bitcast.5, f32[8]{0:T(128)} %bias_ref.1, bf16[2048,1024]{1,0:T(8,128)(2,1)} %wq_hbm.1, bf16[2048,256]{1,0:T(8,128)(2,1)} %wk_hbm.1, bf16[2048,256]{1,0:T(8,128)(2,1)} %wv_hbm.1, bf16[1024,2048]{1,0:T(8,128)(2,1)} %wo_hbm.1), custom_call_target="tpu_custom_call" | custom-call | tf_op jit(solution)/shard_map/layer/pallas_call | solution.py:476
  77.5 1.9 %copy.9 = bf16[2,64,2048]{2,1,0:T(8,128)(2,1)} copy(bf16[2,64,2048]{2,1,0:T(8,128)(2,1)} %bitcast.3) | data formatting | bytes 1048576

commit v3 on v2

--- a/solution.py
+++ b/solution.py
@@ -254,39 +254,53 @@
             arrived(rows_ref.at[j, x * 2 + my_core], recv_x.at[hop - 1, j])
             inside(j, x).start()
 
-    loop(sp_count, relay)
-
-    def finish_rows(j):
-        for x in range(pairs):
-            arrived(rows_ref.at[j, x * 2 + 1 - my_core], recv_p.at[x, j])
-
-    loop(sp_count, finish_rows)
-    for load in loads:
+    def finish_rows(hop):
+        x = at_hop(hop)
+        loop(
+            sp_count,
+            lambda j: arrived(rows_ref.at[j, x * 2 + 1 - my_core], recv_p.at[x, j]),
+        )
+
+    tiles = []
+    for weight, target in ((wk, k_ref), (wv, v_ref), (wq, q_ref)):
+        columns = math.gcd(weight.shape[1], 256)
+        for start in range(0, weight.shape[1], columns):
+            tiles.append((weight, target, slice(start, start + columns)))
+
+    def project(hop, tile):
+        weight, target, at = tile
+        chip = pl.ds(at_hop(hop) * 2, 2)
+        value = jnp.dot(
+            rows_ref[:, chip].reshape(length // pairs, width),
+            weight[:, at],
+            preferred_element_type=jnp.float32,
+        ).astype(jnp.bfloat16)
+        target[:, chip, :, at] = value.reshape(sp_count, 2, part, value.shape[1])
+
+    finish_rows(0)
+    for load in loads[:3]:
         load.wait()
-
-    rows = rows_ref[...].reshape(length, width)
-
-    def project(weight, target):
-        columns = math.gcd(weight.shape[1], 256)
-
-        def tile(n):
-            at = pl.ds(pl.multiple_of(n * columns, columns), columns)
-            target[:, at] = jnp.dot(
-                rows, weight[:, at], preferred_element_type=jnp.float32
-            ).astype(jnp.bfloat16)
-
-        loop(weight.shape[1] // columns, tile)
-
-    project(wk, k_ref)
-    project(wv, v_ref)
-    project(wq, q_ref)
+    for step in range(max(sp_count, len(tiles))):
+        if step < len(tiles):
+            project(0, tiles[step])
+        if step < sp_count:
+            relay(step)
+    for hop in range(1, pairs):
+        finish_rows(hop)
+        for tile in tiles:
+            project(hop, tile)
+    loads[3].wait()
 
     def head(h):
         mine = pl.ds(pl.multiple_of(h * HEAD_DIM, HEAD_DIM), HEAD_DIM)
         shared = pl.ds(pl.multiple_of(h // copies * HEAD_DIM, HEAD_DIM), HEAD_DIM)
-        attend(block, bias_ref[h], q_ref[:, mine], k_ref[:, shared], v_ref[:, shared], att_ref, mine)
-
-    loop(q_ref.shape[1] // HEAD_DIM, head)
+        query_data, key_data, value_data = (
+            ref[:, :, :, at].reshape(length, HEAD_DIM)
+            for ref, at in ((q_ref, mine), (k_ref, shared), (v_ref, shared))
+        )
+        attend(block, bias_ref[h], query_data, key_data, value_data, att_ref, mine)
+
+    loop(q_ref.shape[3] // HEAD_DIM, head)
 
     def chip_copy(j, hop):
         return remote(
@@ -404,6 +418,10 @@
             to_dp(j).wait_send()
 
     loop(sp_count, finish)
+
+
+def below(first, rest):
+    return jnp.concatenate((first, rest), axis=0) if rest.shape[0] else first
 
 
 def attend(block, bias, query_data, key_data, value_data, o_ref, columns):
@@ -418,45 +436,42 @@
     at_row = lax.broadcasted_iota(jnp.int32, (block, block), 0)
     at_col = lax.broadcasted_iota(jnp.int32, (block, block), 1)
     causal = at_col < at_row
-    for r in range(length // block):
-        rows = slice(r * block, (r + 1) * block)
-        query = query_data[rows]
-        carried = None
-        total = None
-        for c in range(r, -1, -1):
-            keys = slice(c * block, (c + 1) * block)
-            scores = (
-                lax.dot_general(
-                    query,
-                    key_data[keys],
-                    (((1,), (1,)), ((), ())),
-                    preferred_element_type=jnp.float32,
-                )
-                * scale
-                + bias
+    carried = None
+    total = None
+    for c in range(length // block - 1, -1, -1):
+        keys = slice(c * block, (c + 1) * block)
+        scores = (
+            lax.dot_general(
+                query_data[c * block :],
+                key_data[keys],
+                (((1,), (1,)), ((), ())),
+                preferred_element_type=jnp.float32,
             )
-            soft = jnp.log2(1.0 + jnp.exp2(-jnp.abs(scores)))
-            log_keep = -jnp.maximum(scores, 0.0) - soft
-            log_break = jnp.minimum(scores, 0.0) - soft
-            if c == r:
-                log_keep = jnp.where(causal, log_keep, 0.0)
-            high = log_keep.astype(jnp.bfloat16)
-            low = (log_keep - high.astype(jnp.float32)).astype(jnp.bfloat16)
-            sums = jnp.dot(
-                jnp.concatenate((high, low), axis=1), summing, preferred_element_type=jnp.float32
-            )
-            exponent = log_break + sums[:, :block]
-            if carried is not None:
-                exponent = exponent + carried
-            weights = jnp.exp2(exponent)
-            if c == r:
-                weights = jnp.where(causal, weights, 0.0)
-            term = jnp.dot(
-                weights.astype(jnp.bfloat16), value_data[keys], preferred_element_type=jnp.float32
-            )
-            carried = sums[:, block:] if carried is None else carried + sums[:, block:]
-            total = term if total is None else total + term
-        o_ref[rows, columns] = total.astype(jnp.bfloat16)
+            * scale
+            + bias
+        )
+        soft = jnp.log2(1.0 + jnp.exp2(-jnp.abs(scores)))
+        log_keep = -jnp.maximum(scores, 0.0) - soft
+        log_break = jnp.minimum(scores, 0.0) - soft
+        log_keep = below(jnp.where(causal, log_keep[:block], 0.0), log_keep[block:])
+        high = log_keep.astype(jnp.bfloat16)
+        low = (log_keep - high.astype(jnp.float32)).astype(jnp.bfloat16)
+        sums = jnp.dot(
+            jnp.concatenate((high, low), axis=1), summing, preferred_element_type=jnp.float32
+        )
+        exponent = log_break + sums[:, :block]
+        if carried is None:
+            carried = sums[:, block:]
+        else:
+            exponent = below(exponent[:block], exponent[block:] + carried)
+            carried = below(sums[:block, block:], sums[block:, block:] + carried)
+        weights = jnp.exp2(exponent)
+        weights = below(jnp.where(causal, weights[:block], 0.0), weights[block:])
+        term = jnp.dot(
+            weights.astype(jnp.bfloat16), value_data[keys], preferred_element_type=jnp.float32
+        )
+        total = term if total is None else below(term[:block], term[block:] + total)
+    o_ref[:, columns] = total.astype(jnp.bfloat16)
 
 
 def gathered(tokens, norm_gain, w_query, w_key, w_value, break_bias, w_out):
@@ -486,9 +501,9 @@
             room(dp_count, own, part, width),
             room(dp_count, own, part, width),
             room(sp_count, dp_count, part, width),
-            room(length, w_query.shape[1]),
-            room(length, w_key.shape[1]),
-            room(length, w_value.shape[1]),
+            room(sp_count, dp_count, part, w_query.shape[1]),
+            room(sp_count, dp_count, part, w_key.shape[1]),
+            room(sp_count, dp_count, part, w_value.shape[1]),
             room(length, w_query.shape[1]),
             room(sp_count, dp_count, part, width),
             room(pairs, sp_count, part, width),

time: 79.5 us -> 74.3 us (0.935)
  the two profiles are of different devices: /device:TPU:29 before, /device:TPU:31 now
where the time goes in v3:
time: 74.3 us; the launch traced here: 74.1 us
  Pallas kernels  72.2 us (97%)
  local copies, waits for them, and re-layouts  1.88 us (3%)
    pallas_call x1, Pallas kernels, gathered(): pl.pallas_call(functools.partial(layer_kernel, sp_count, dp_count, copies...  72.2 us
    unnamed x1, local copies, waits for them, and re-layouts  1.88 us

profile of v3, /device:TPU:31, one launch (start us, length us, event | category | flops | bytes accessed | tf_op | source)
XLA Modules:
  0.0 74.1 jit_solution(5522026846792224438)
XLA Ops:
  0.0 72.2 %layer.1 = bf16[2,4,16,2048]{3,2,1,0:T(8,128)(2,1)} custom-call(bf16[2,4,16,2048]{3,2,1,0:T(8,128)(2,1)} %bitcast.4, f32[1,2048]{1,0:T(1,128)} %bitcast.5, f32[8]{0:T(128)} %bias_ref.1, bf16[2048,1024]{1,0:T(8,128)(2,1)} %wq_hbm.1, bf16[2048,256]{1,0:T(8,128)(2,1)} %wk_hbm.1, bf16[2048,256]{1,0:T(8,128)(2,1)} %wv_hbm.1, bf16[1024,2048]{1,0:T(8,128)(2,1)} %wo_hbm.1), custom_call_target="tpu_custom_call" | custom-call | tf_op jit(solution)/shard_map/layer/pallas_call | solution.py:491
  72.3 1.9 %copy.9 = bf16[2,64,2048]{2,1,0:T(8,128)(2,1)} copy(bf16[2,64,2048]{2,1,0:T(8,128)(2,1)} %bitcast.3) | data formatting | bytes 1048576

commit v4 on v3

--- a/solution.py
+++ b/solution.py
@@ -323,37 +323,38 @@
         )
 
     hops = list(range(1, pairs)) + [0]
-    some = math.gcd(sp_count, 2)
-    group = sp_count // some
     wide = math.gcd(width, 512)
-    tall = group * dp_count * part
-
-    def send_sums(j):
+
+    def turn(step):
+        return lax.rem(my_sp + step, sp_count)
+
+    def send_sums(step):
+        j = turn(step)
         for hop in range(1, pairs):
             chip_copy(j, hop).wait_recv()
             mine = p_ref[j, at_hop(hop) * 2 + my_core].astype(jnp.float32)
             summed[hop - 1, j] = (mine + from_core[hop, j].astype(jnp.float32)).astype(jnp.bfloat16)
             sum_copy(j, hop).start()
 
-    for r in range(some):
-        heads = att_ref[r * tall : (r + 1) * tall, :]
+    for hop in hops:
+        chip = pl.ds(at_hop(hop) * 2, 2)
+        heads = att_ref[:, chip].reshape(length // pairs, att_ref.shape[3])
 
         def out_tile(n):
             at = pl.ds(pl.multiple_of(n * wide, wide), wide)
             value = jnp.dot(heads, wo[:, at], preferred_element_type=jnp.float32)
-            p_ref[r * group : (r + 1) * group, :, :, at] = value.astype(jnp.bfloat16).reshape(
-                group, dp_count, part, wide
-            )
+            p_ref[:, chip, :, at] = value.astype(jnp.bfloat16).reshape(sp_count, 2, part, wide)
 
         loop(width // wide, out_tile)
-        for hop in hops:
-            loop(group, lambda j: chip_copy(r * group + j, hop).start())
-        loop(group, lambda j: send_sums(r * group + j))
+        loop(sp_count, lambda step: chip_copy(turn(step), hop).start())
+        if hop == pairs - 1:
+            loop(sp_count, send_sums)
 
     def to_sp(j):
         return remote(done.at[j], home.at[my_sp], send_3.at[j], recv_3.at[my_sp], j, my_dp)
 
-    def complete(j):
+    def complete(step):
+        j = turn(step)
         chip_copy(j, 0).wait_recv()
         total = p_ref[j, my_dp].astype(jnp.float32) + from_core[0, j].astype(jnp.float32)
         for hop in range(1, pairs):
@@ -369,7 +370,6 @@
         def _():
             pltpu.make_async_copy(done.at[j], home.at[my_sp], recv_3.at[my_sp]).start()
 
-    loop(sp_count, complete)
 
     def to_dp(i):
         e, s = i // own, lax.rem(i, own)
@@ -380,7 +380,8 @@
     def is_mine(i):
         return i // own == my_dp
 
-    def send_home(i):
+    def send_home(step):
+        i = lax.rem(my_sp - step + sp_count, sp_count)
         arrived(home.at[i], recv_3.at[i])
 
         @pl.when(jnp.logical_not(is_mine(i)))
@@ -392,7 +393,15 @@
             s = lax.rem(i, own)
             pltpu.make_async_copy(home.at[i], out_ref.at[s, my_dp], recv_4.at[s, my_dp]).start()
 
-    loop(sp_count, send_home)
+    lag = min(2, sp_count)
+    loop(lag, complete)
+
+    def both(step):
+        complete(step + lag)
+        send_home(step)
+
+    loop(sp_count - lag, both)
+    loop(lag, lambda step: send_home(step + sp_count - lag))
     for s in range(own):
         for q in range(dp_count):
             arrived(out_ref.at[s, q], recv_4.at[s, q])
@@ -471,7 +480,7 @@
             weights.astype(jnp.bfloat16), value_data[keys], preferred_element_type=jnp.float32
         )
         total = term if total is None else below(term[:block], term[block:] + total)
-    o_ref[:, columns] = total.astype(jnp.bfloat16)
+    o_ref[:, :, :, columns] = total.astype(jnp.bfloat16).reshape(*o_ref.shape[:3], HEAD_DIM)
 
 
 def gathered(tokens, norm_gain, w_query, w_key, w_value, break_bias, w_out):
@@ -504,7 +513,7 @@
             room(sp_count, dp_count, part, w_query.shape[1]),
             room(sp_count, dp_count, part, w_key.shape[1]),
             room(sp_count, dp_count, part, w_value.shape[1]),
-            room(length, w_query.shape[1]),
+            room(sp_count, dp_count, part, w_query.shape[1]),
             room(sp_count, dp_count, part, width),
             room(pairs, sp_count, part, width),
             room(pairs - 1, sp_count, part, width),

time: 74.3 us -> 74.9 us (level)
  the two profiles are of different devices: /device:TPU:31 before, /device:TPU:0 now
where the time goes in v4:
time: 74.9 us; the launch traced here: 74.7 us
  Pallas kernels  72.8 us (97%)
  local copies, waits for them, and re-layouts  1.88 us (3%)
    pallas_call x1, Pallas kernels, gathered(): pl.pallas_call(functools.partial(layer_kernel, sp_count, dp_count, copies...  72.8 us
    unnamed x1, local copies, waits for them, and re-layouts  1.88 us

profile of v4, /device:TPU:0, one launch (start us, length us, event | category | flops | bytes accessed | tf_op | source)
XLA Modules:
  0.0 74.7 jit_solution(11633505657705956175)
XLA Ops:
  0.0 72.8 %layer.1 = bf16[2,4,16,2048]{3,2,1,0:T(8,128)(2,1)} custom-call(bf16[2,4,16,2048]{3,2,1,0:T(8,128)(2,1)} %bitcast.4, f32[1,2048]{1,0:T(1,128)} %bitcast.5, f32[8]{0:T(128)} %bias_ref.1, bf16[2048,1024]{1,0:T(8,128)(2,1)} %wq_hbm.1, bf16[2048,256]{1,0:T(8,128)(2,1)} %wk_hbm.1, bf16[2048,256]{1,0:T(8,128)(2,1)} %wv_hbm.1, bf16[1024,2048]{1,0:T(8,128)(2,1)} %wo_hbm.1), custom_call_target="tpu_custom_call" | custom-call | tf_op jit(solution)/shard_map/layer/pallas_call | solution.py:500
  72.9 1.9 %copy.9 = bf16[2,64,2048]{2,1,0:T(8,128)(2,1)} copy(bf16[2,64,2048]{2,1,0:T(8,128)(2,1)} %bitcast.3) | data formatting | bytes 1048576
